TPU v7x, 32 devices: a whole 2x2x4 slice. The times are simulated.
32 devices in a mesh: ep: 16 (over z, x, core), tp: 2 (over y).
Axes of the slice: x: 2, y: 2, z: 4, core: 2. Of those that a mesh axis runs over, the one named last changes fastest.
Arguments:
- tokens: bfloat16 [192, 4096], P('ep', 'tp')
- norm_gain: float32 [4096], P('tp'), may hold values from 0.1 to 1.9
- routes: int32 [192, 6], P('ep'), may hold values from 0 to 15, all different within a row; in each aligned block of 12 rows (0 to 11, 12 to 23, ...) at most 5 rows name the same one
- route_weights: float32 [192, 6], P('ep'), may hold values from 0.05 to 1
- expert_gate: bfloat16 [16, 4096, 1024], P('ep', 'tp'), may hold values from -0.09375 to 0.09375
- expert_up: bfloat16 [16, 4096, 1024], P('ep', 'tp'), may hold values from -0.09375 to 0.09375
- expert_down: bfloat16 [16, 1024, 4096], P('ep', None, 'tp'), may hold values from -0.1875 to 0.1875
- shared_gate: bfloat16 [4096, 1024], P('tp'), may hold values from -0.09375 to 0.09375
- shared_up: bfloat16 [4096, 1024], P('tp'), may hold values from -0.09375 to 0.09375
- shared_down: bfloat16 [1024, 4096], P(None, 'tp'), may hold values from -0.1875 to 0.1875
Outputs:
- mixed: bfloat16 [192, 4096], P('ep', 'tp')
Inputs may be any that keep to these rules, and one draw needn't show every extreme that they name: `routes`: each row names 6 different experts; among the rows of one device no expert is named more than 5 times, and in some devices' rows one expert is named exactly 5 times.
All inputs are finite; a program needn't handle non-finite values.
Results may differ from a plain program's by a relative error of at most 0.0068.
Values may be sent and summed in bfloat16 or wider, within the bound.
A program may use at most 64 MiB of HBM per device.

v0:
```python
import functools

import jax
import jax.numpy as jnp
from jax import lax
from jax.experimental import pallas as pl
from jax.experimental.pallas import tpu as pltpu
from jax.sharding import PartitionSpec as P

MESH = pl.DeviceIdType.MESH
F32 = jnp.float32
BF16 = jnp.bfloat16
LANES = 128
TN = (((0,), (0,)), ((), ()))
SPLIT = True
HILO = True


def silu_mul(g, u):
    return g / (1.0 + jnp.exp(-g)) * u


def kernel(
    n, tp, cap, chunks, pieces,
    x_ref, gain_ref, routes_ref, rw_ref,
    eg_hbm, eu_hbm, ed_hbm, sg_hbm, su_hbm, sd_hbm,
    out_ref,
    wg, wu, wd, vg, vu, vd,
    packed, outbuf, arrive, retbuf, back,
    rows, sssend, ssrecv, shsend, shrecv, acc, shout,
    wsem, dsend, drecv, rsend, rrecv, tsend, trecv, qsend, qrecv, hsend, hrecv,
    *exchanged,
):
    me = lax.axis_index("ep")
    my_tp = lax.axis_index("tp")
    toks, width = x_ref.shape
    picks = routes_ref.shape[0]
    ff = wg.shape[1]
    fs = vg.shape[1]
    blocks = width // LANES
    jc = blocks * cap
    n_rows = cap * n
    mine, psend, precv = exchanged[0::3], exchanged[1::3], exchanged[2::3]
    cols = ff // chunks

    barrier = pltpu.get_barrier_semaphore()
    for i in range(1, n):
        pl.semaphore_signal(barrier, inc=1, device_id={"ep": lax.rem(me + i, n)}, device_id_type=MESH)
    for i in range(1, tp):
        pl.semaphore_signal(barrier, inc=1, device_id={"tp": lax.rem(my_tp + i, tp)}, device_id_type=MESH)

    loads = {}
    slot = 0
    for name, src, dst in (
        ("sg", sg_hbm, vg), ("su", su_hbm, vu), ("sd", sd_hbm, vd),
        ("eg", eg_hbm.at[0], wg), ("eu", eu_hbm.at[0], wu), ("ed", ed_hbm.at[0], wd),
    ):
        depth = dst.shape[0] // pieces
        loads[name] = []
        for i in range(pieces):
            c = pltpu.make_async_copy(
                src.at[pl.ds(i * depth, depth)], dst.at[pl.ds(i * depth, depth)], wsem.at[slot]
            )
            c.start()
            loads[name].append(c)
            slot += 1

    routes = routes_ref[...]
    rw = rw_ref[...]
    scaled = 2.5 * rw / jnp.sum(rw, axis=0, keepdims=True)
    expert = lax.broadcasted_iota(jnp.int32, (n, toks), 0)
    named = jnp.zeros((n, toks), F32)
    weight = jnp.zeros((n, toks), F32)
    for k in range(picks):
        hit = routes[k : k + 1, :] == expert
        named = named + jnp.where(hit, 1.0, 0.0)
        weight = weight + jnp.where(hit, scaled[k : k + 1, :], 0.0)
    row_i = lax.broadcasted_iota(jnp.int32, (toks, toks), 0)
    col_i = lax.broadcasted_iota(jnp.int32, (toks, toks), 1)
    earlier = jnp.where(row_i < col_i, 1.0, 0.0).astype(BF16)
    before = jnp.dot(named.astype(BF16), earlier, preferred_element_type=F32)
    place = jnp.where(named > 0.5, before, -1.0)
    w_hi = weight.astype(BF16).astype(F32)
    w_lo = weight - w_hi

    def by_slot(v):
        return jnp.concatenate([jnp.where(place == s, v, 0.0) for s in range(cap)], axis=0).astype(BF16)

    select, comb_hi, comb_lo = by_slot(1.0), by_slot(w_hi), by_slot(w_lo)

    def pack(value, j, m):
        for s in range(cap):
            packed[pl.ds(j * cap + s, m, stride=jc), :] = value[s * m : (s + 1) * m, :]

    def unpack(j, m):
        return jnp.concatenate(
            [packed[pl.ds(j * cap + s, m, stride=jc), :] for s in range(cap)], axis=0
        )

    x = x_ref[...]
    for j in range(blocks):
        cut = slice(j * LANES, (j + 1) * LANES)
        pack(jnp.dot(select, x[:, cut], preferred_element_type=F32), j, n)
    for p in range(n):
        outbuf[p] = packed[pl.ds(p * jc, jc), :].astype(BF16)

    pl.semaphore_wait(barrier, n - 1 + tp - 1)

    def to_tp(src, dst_of, send_of, recv_of):
        copies = []
        for i in range(1, tp):
            c = pltpu.make_async_remote_copy(
                src_ref=src, dst_ref=dst_of(i - 1), send_sem=send_of(i - 1), recv_sem=recv_of(i - 1),
                device_id={"tp": lax.rem(my_tp + i, tp)}, device_id_type=MESH,
            )
            c.start()
            copies.append(c)
        return copies

    quarter = n // 4
    q, inner = me // quarter, lax.rem(me, quarter)
    half, bit = q // 2, lax.rem(q, 2)
    near = (q, 2 * half + 1 - bit)
    far = (2 * (1 - half) + bit, 2 * (1 - half) + 1 - bit)

    def members(quarters):
        return [qt * quarter + lax.rem(inner + i, quarter) for qt in quarters for i in range(quarter)]

    groups = [members(near)] + [members((f,)) for f in far] if SPLIT else [members(near), members(far)]

    def copy_to(src, dst, send, recv, to):
        return pltpu.make_async_remote_copy(
            src_ref=src.at[to], dst_ref=dst.at[me], send_sem=send.at[to], recv_sem=recv.at[me],
            device_id={"ep": to}, device_id_type=MESH,
        )

    def wait_from(src, dst, send, recv, frm):
        pltpu.make_async_remote_copy(
            src_ref=src.at[frm], dst_ref=dst.at[frm], send_sem=send.at[frm], recv_sem=recv.at[frm],
            device_id={"ep": frm}, device_id_type=MESH,
        ).wait_recv()

    pending = []

    def send_group(g, src, dst, send, recv):
        for i, to in enumerate(groups[g]):
            if g or i:
                c = copy_to(src, dst, send, recv, to)
                c.start()
                pending.append(c)

    def wait_group(g, src, dst, send, recv):
        for i, frm in enumerate(groups[g]):
            if g or i:
                wait_from(src, dst, send, recv, frm)

    for g in range(len(groups)):
        send_group(g, outbuf, arrive, dsend, drecv)
    arrive[me] = outbuf[me]

    xf = x.astype(F32)
    gain = gain_ref[...]
    xg = (xf * gain).astype(BF16)
    ss_own = jnp.sum(xf * xf, axis=1, keepdims=True)
    shsend[...] = jnp.zeros(shsend.shape, F32)
    shsend[0:toks, 2 * fs : 2 * fs + LANES] = jnp.broadcast_to(ss_own, (toks, LANES))
    for name, w, base in (("sg", vg, 0), ("su", vu, fs)):
        for c in loads[name]:
            c.wait()
        shsend[0:toks, base : base + fs] = jnp.dot(xg, w[...], preferred_element_type=F32)
    shcopies = to_tp(shsend, lambda i: shrecv.at[i], lambda i: hsend.at[i], lambda i: hrecv.at[i])
    pending.extend(shcopies)
    def finish_shared():
        for c in loads["sd"]:
            c.wait()
        for c in shcopies:
            c.wait_recv()
        total = shsend[...]
        for i in range(tp - 1):
            total = total + shrecv[i]
        r_own = lax.rsqrt(total[:, 2 * fs : 2 * fs + 1] / (width * tp) + 1e-06)
        sh_hidden = silu_mul(total[:, 0:fs] * r_own, total[:, fs : 2 * fs] * r_own).astype(BF16)
        shout[...] = jnp.dot(sh_hidden, vd[...], preferred_element_type=F32)

    def first_half(g):
        m = len(groups[g])
        count, base = m * cap, starts[g]
        low = -(-count // 16) * 16
        wait_group(g, outbuf, arrive, dsend, drecv)
        for i, p in enumerate(groups[g]):
            packed[pl.ds(i * jc, jc), :] = arrive[p].astype(F32)
        ss = jnp.zeros((count, LANES), F32)
        for j in range(blocks):
            cut = slice(j * LANES, (j + 1) * LANES)
            piece = unpack(j, m)
            ss = ss + piece * piece
            scaled_piece = piece * gain[:, cut]
            hi = scaled_piece.astype(BF16)
            rows[0:count, cut] = hi
            if HILO:
                rows[low : low + count, cut] = (scaled_piece - hi.astype(F32)).astype(BF16)
        sssend[base : base + count] = jnp.broadcast_to(jnp.sum(ss, axis=1, keepdims=True), (count, LANES))
        part = pl.ds(base, count)
        copies = to_tp(
            sssend.at[part], lambda i: ssrecv.at[i, part],
            lambda i: qsend.at[i * len(groups) + g], lambda i: qrecv.at[i * len(groups) + g],
        )
        all_copies = [copies]
        pending.extend(copies)
        taken_rows = rows[0 : 2 * low, :] if HILO else rows[0:count, :]
        for c in range(chunks):
            cut = slice(c * cols, (c + 1) * cols)
            for w, at in ((wg, 0), (wu, cols)):
                v = jnp.dot(taken_rows, w[:, cut], preferred_element_type=F32)
                if HILO:
                    v = v[0:count] + v[low : low + count]
                mine[g][c, :, at : at + cols] = v
                psend[g][c, :, at : at + cols] = v.astype(BF16)
            at_sem = lambda i: (i * len(groups) + g) * chunks + c
            copies = to_tp(
                psend[g].at[c], lambda i: precv[g].at[i, c],
                lambda i: tsend.at[at_sem(i)], lambda i: trecv.at[at_sem(i)],
            )
            all_copies.append(copies)
            pending.extend(copies)
        return all_copies

    def second_half(g, all_copies):
        m = len(groups[g])
        count, base = m * cap, starts[g]
        for c in all_copies[0]:
            c.wait_recv()
        ss_all = sssend[base : base + count, :]
        for i in range(tp - 1):
            ss_all = ss_all + ssrecv[i, base : base + count, :]
        r = lax.rsqrt(ss_all[:, 0:1] / (width * tp) + 1e-06)
        for c in range(chunks):
            for copy in all_copies[1 + c]:
                copy.wait_recv()
            both = mine[g][c]
            for i in range(tp - 1):
                both = both + precv[g][i, c].astype(F32)
            hidden = silu_mul(both[:, 0:cols] * r, both[:, cols : 2 * cols] * r).astype(BF16)
            part = jnp.dot(hidden, wd[c * cols : (c + 1) * cols, :], preferred_element_type=F32)
            if c == 0:
                acc[0:count, :] = part
            elif c < chunks - 1:
                acc[0:count, :] += part
            else:
                for j in range(blocks):
                    cut = slice(j * LANES, (j + 1) * LANES)
                    pack(acc[0:count, cut] + part[:, cut], j, m)
        for i, p in enumerate(groups[g]):
            retbuf[p] = packed[pl.ds(i * jc, jc), :].astype(BF16)
        send_group(g, retbuf, back, rsend, rrecv)

    starts = []
    for g in range(len(groups)):
        starts.append(sum(-(-len(groups[i]) * cap // 8) * 8 for i in range(g)))
    if HILO:
        rows[...] = jnp.zeros(rows.shape, BF16)
    for name in ("eg", "eu"):
        for c in loads[name]:
            c.wait()
    states = [first_half(0)]
    finish_shared()
    for c in loads["ed"]:
        c.wait()
    if len(groups) == 3:
        states.append(first_half(1))
        second_half(0, states[0])
        states.append(first_half(2))
    else:
        states.append(first_half(1))
        second_half(0, states[0])
    back[me] = retbuf[me]
    for g in range(1, len(groups)):
        second_half(g, states[g])
    for g in range(len(groups)):
        wait_group(g, retbuf, back, rsend, rrecv)
    for p in range(n):
        packed[pl.ds(p * jc, jc), :] = back[p].astype(F32)
    for j in range(blocks):
        cut = slice(j * LANES, (j + 1) * LANES)
        piece = unpack(j, n).astype(BF16)
        routed = lax.dot_general(comb_hi, piece, TN, preferred_element_type=F32)
        routed = routed + lax.dot_general(comb_lo, piece, TN, preferred_element_type=F32)
        out_ref[:, cut] = (shout[0:toks, cut] + routed).astype(BF16)
    for c in pending:
        c.wait_send()


def local(tokens, norm_gain, routes, route_weights, eg, eu, ed, sg, su, sd):
    toks, width = tokens.shape
    picks = routes.shape[1]
    n, tp = lax.axis_size("ep"), lax.axis_size("tp")
    cap = max(2, toks * picks // n + 1)
    ff, fs = eg.shape[2], sg.shape[1]
    chunks, pieces = 2, 4
    jc = width // LANES * cap
    n_rows = n * cap
    padded = -(-toks // 16) * 16
    cols = ff // chunks
    others = max(1, tp - 1)
    sizes = [n // 2, n // 4, n // 4] if SPLIT else [n // 2, n // 2]
    exchanged = []
    for m in sizes:
        exchanged += [
            pltpu.VMEM((chunks, m * cap, 2 * cols), F32),
            pltpu.VMEM((chunks, m * cap, 2 * cols), BF16),
            pltpu.VMEM((others, chunks, m * cap, 2 * cols), BF16),
        ]
    vmem = pl.BlockSpec(memory_space=pltpu.VMEM)
    hbm = pl.BlockSpec(memory_space=pl.ANY)
    dma = pltpu.SemaphoreType.DMA
    return pl.pallas_call(
        functools.partial(kernel, n, tp, cap, chunks, pieces),
        out_shape=jax.ShapeDtypeStruct((toks, width), BF16),
        in_specs=[vmem] * 4 + [hbm] * 6,
        out_specs=vmem,
        scratch_shapes=[
            pltpu.VMEM((width, ff), BF16), pltpu.VMEM((width, ff), BF16), pltpu.VMEM((ff, width), BF16),
            pltpu.VMEM((width, fs), BF16), pltpu.VMEM((width, fs), BF16), pltpu.VMEM((fs, width), BF16),
            pltpu.VMEM((n * jc, LANES), F32),
            pltpu.VMEM((n, jc, LANES), BF16), pltpu.VMEM((n, jc, LANES), BF16),
            pltpu.VMEM((n, jc, LANES), BF16), pltpu.VMEM((n, jc, LANES), BF16),
            pltpu.VMEM((2 * n_rows, width), BF16),
            pltpu.VMEM((2 * n_rows, LANES), F32), pltpu.VMEM((others, 2 * n_rows, LANES), F32),
            pltpu.VMEM((padded, 2 * fs + LANES), F32), pltpu.VMEM((others, padded, 2 * fs + LANES), F32),
            pltpu.VMEM((n_rows, width), F32), pltpu.VMEM((padded, width), F32),
            dma((6 * pieces,)),
            dma((n,)), dma((n,)), dma((n,)), dma((n,)),
            dma((others * chunks * len(sizes),)), dma((others * chunks * len(sizes),)),
            dma((others * len(sizes),)), dma((others * len(sizes),)), dma((others,)), dma((others,)),
        ] + exchanged,
        compiler_params=pltpu.CompilerParams(
            collective_id=0, has_side_effects=True, vmem_limit_bytes=60 * 1024 * 1024
        ),
    )(tokens, norm_gain.reshape(1, width), routes.T, route_weights.T, eg, eu, ed, sg, su, sd)


def solution(mesh):
    placed = (
        P("ep", "tp"),
        P("tp"),
        P("ep", None),
        P("ep", None),
        P("ep", "tp", None),
        P("ep", "tp", None),
        P("ep", None, "tp"),
        P("tp", None),
        P("tp", None),
        P(None, "tp"),
    )
    return jax.shard_map(
        local, mesh=mesh, in_specs=placed, out_specs=P("ep", "tp"), check_vma=False
    )
```

profile of v0, /device:TPU:0, one launch (start us, length us, event | category | flops | bytes accessed | tf_op | source)
XLA Modules:
  0.0 33.2 jit_solution(8828738656699796394)
XLA Ops:
  0.0 31.7 %shard_map.100 = bf16[12,2048]{1,0:T(8,128)(2,1)} custom-call(bf16[12,2048]{1,0:T(8,128)(2,1)} %x_ref.1, f32[1,2048]{1,0:T(1,128)} %bitcast.3, s32[6,12]{1,0:T(8,128)} %bitcast.4, f32[6,12]{1,0:T(8,128)} %bitcast.5, bf16[1,2048,1024]{2,1,0:T(8,128)(2,1)} %eg_hbm.1, bf16[1,2048,1024]{2,1,0:T(8,128)(2,1)} %eu_hbm.1, bf16[1,1024,2048]{2,1,0:T(8,128)(2,1)} %ed_hbm.1, ...), custom_call_target="tpu_custom_call" | custom-call | tf_op jit(solution)/shard_map/pallas_call | solution.py:316
  31.7 1.5 %copy.12 = bf16[12,2048]{1,0:T(8,128)(2,1)} copy(bf16[12,2048]{1,0:T(8,128)(2,1)} %shard_map.100) | data formatting | bytes 98304
where the time goes:
time: 33.4 us; the launch traced here: 33.2 us
  Pallas kernels  31.7 us (95%)
  local copies, waits for them, and re-layouts  1.47 us (4%)
    pallas_call x1, Pallas kernels, local(): pl.pallas_call(functools.partial(kernel, n, tp, cap, chunks, pieces), out...  31.7 us
    unnamed x1, local copies, waits for them, and re-layouts  1.47 us

commit v1 on v0

v1 whole, which is shorter than its diff:
```python
import functools

import jax
import jax.numpy as jnp
from jax import lax
from jax.experimental import pallas as pl
from jax.experimental.pallas import tpu as pltpu
from jax.sharding import PartitionSpec as P

MESH = pl.DeviceIdType.MESH
F32 = jnp.float32
BF16 = jnp.bfloat16
LANES = 128
TN = (((0,), (0,)), ((), ()))


def silu_mul(g, u):
    return g / (1.0 + jnp.exp(-g)) * u


def kernel(
    n, tp, cap, chunks, pieces,
    x_hbm, gain_hbm, routes_hbm, rw_hbm,
    eg_hbm, eu_hbm, ed_hbm, sg_hbm, su_hbm, sd_hbm,
    out_ref,
    wg, wu, wd, vg, vu, vd,
    x_ref, gain_ref, routes_ref, rw_ref, xm_ref, meta, metam,
    packed, outbuf, arrive, retbuf, back,
    rows, sssend, ssrecv, shsend, shrecv, acc, shout,
    isem, wsem, dsend, drecv, rsend, rrecv, tsend, trecv, qsend, qrecv, hsend, hrecv, xsend, xrecv,
    *exchanged,
):
    me = lax.axis_index("ep")
    my_tp = lax.axis_index("tp")
    m, quarter = n // 2, n // 4
    half, inner = me // m, lax.rem(me, m)
    mirror = lax.rem(me + m, n)
    spot = lax.rem(me, quarter)
    toks, width = x_ref.shape
    picks = routes_ref.shape[0]
    ff = wg.shape[1]
    fs = vg.shape[1]
    blocks = width // LANES
    jc = blocks * cap
    cols = ff // chunks
    mine, psend, precv = exchanged[0::3], exchanged[1::3], exchanged[2::3]

    def mate(i):
        return half * m + lax.rem(inner + i, m)

    def in_quarter(q):
        return [q * quarter + lax.rem(spot + i, quarter) for i in range(quarter)]

    near = [mate(i) for i in range(m)]
    groups = [near, in_quarter(2 * (1 - half)), in_quarter(2 * (1 - half) + 1)]

    barrier = pltpu.get_barrier_semaphore()
    pl.semaphore_signal(barrier, inc=1, device_id={"ep": mirror}, device_id_type=MESH)
    for i in range(1, m):
        pl.semaphore_signal(barrier, inc=1, device_id={"ep": mate(i)}, device_id_type=MESH)
    for i in range(1, tp):
        pl.semaphore_signal(barrier, inc=1, device_id={"tp": lax.rem(my_tp + i, tp)}, device_id_type=MESH)

    small = []
    for i, (src, dst) in enumerate(
        ((routes_hbm, routes_ref), (rw_hbm, rw_ref), (x_hbm, x_ref), (gain_hbm, gain_ref))
    ):
        c = pltpu.make_async_copy(src, dst, isem.at[i])
        c.start()
        small.append(c)
    for c in small:
        c.wait()
    loads = {}
    slot = 0
    for name, src, dst in (
        ("eg", eg_hbm.at[0], wg), ("eu", eu_hbm.at[0], wu), ("sg", sg_hbm, vg), ("su", su_hbm, vu),
        ("ed", ed_hbm.at[0], wd), ("sd", sd_hbm, vd),
    ):
        depth = dst.shape[0] // pieces
        loads[name] = []
        for i in range(pieces):
            c = pltpu.make_async_copy(
                src.at[pl.ds(i * depth, depth)], dst.at[pl.ds(i * depth, depth)], wsem.at[slot]
            )
            c.start()
            loads[name].append(c)
            slot += 1

    def loaded(*names):
        for name in names:
            for c in loads[name]:
                c.wait()

    def places(routes, base, number):
        expert = lax.broadcasted_iota(jnp.int32, (number, toks), 0) + base
        hits = [routes[k : k + 1, :] == expert for k in range(picks)]
        named = jnp.zeros((number, toks), F32)
        for hit in hits:
            named = named + jnp.where(hit, 1.0, 0.0)
        row_i = lax.broadcasted_iota(jnp.int32, (toks, toks), 0)
        col_i = lax.broadcasted_iota(jnp.int32, (toks, toks), 1)
        earlier = jnp.where(row_i < col_i, 1.0, 0.0).astype(BF16)
        before = jnp.dot(named.astype(BF16), earlier, preferred_element_type=F32)
        return hits, jnp.where(named > 0.5, before, -1.0)

    def by_slot(place, v):
        return jnp.concatenate([jnp.where(place == s, v, 0.0) for s in range(cap)], axis=0).astype(BF16)

    def pack(value, j, number):
        for s in range(cap):
            packed[pl.ds(j * cap + s, number, stride=jc), :] = value[s * number : (s + 1) * number, :]

    def unpack(j, number):
        return jnp.concatenate(
            [packed[pl.ds(j * cap + s, number, stride=jc), :] for s in range(cap)], axis=0
        )

    def select_rows(g, routes, x):
        select = by_slot(places(routes, half * m, m)[1], 1.0)
        for j in range(blocks):
            cut = slice(j * LANES, (j + 1) * LANES)
            pack(jnp.dot(select, x[:, cut], preferred_element_type=F32), j, m)
        for p in range(m):
            outbuf[g, p] = packed[pl.ds(p * jc, jc), :].astype(BF16)

    pending = []

    def to_tp(src, dst_of, send_of, recv_of):
        copies = []
        for i in range(1, tp):
            c = pltpu.make_async_remote_copy(
                src_ref=src, dst_ref=dst_of(i - 1), send_sem=send_of(i - 1), recv_sem=recv_of(i - 1),
                device_id={"tp": lax.rem(my_tp + i, tp)}, device_id_type=MESH,
            )
            c.start()
            copies.append(c)
        pending.extend(copies)
        return copies

    def to_mirror(src, dst, at):
        c = pltpu.make_async_remote_copy(
            src_ref=src, dst_ref=dst, send_sem=xsend.at[at], recv_sem=xrecv.at[at],
            device_id={"ep": mirror}, device_id_type=MESH,
        )
        c.start()
        pending.append(c)
        return c

    def send_tokens(g, home):
        for i in range(1, m):
            to = lax.rem(inner + i, m)
            c = pltpu.make_async_remote_copy(
                src_ref=outbuf.at[g, to], dst_ref=arrive.at[home], send_sem=dsend.at[g, to], recv_sem=drecv.at[home],
                device_id={"ep": mate(i)}, device_id_type=MESH,
            )
            c.start()
            pending.append(c)
        arrive[home] = outbuf[g, inner]

    def wait_tokens(g):
        for i, home in enumerate(groups[g]):
            if g == 0 and i == 0:
                continue
            copy = pltpu.make_async_remote_copy(
                src_ref=outbuf.at[0, 0], dst_ref=arrive.at[home], send_sem=dsend.at[0, 0], recv_sem=drecv.at[home],
                device_id={"ep": mate(1)}, device_id_type=MESH,
            )
            if g == 0:
                copy.wait_recv()
            else:
                @pl.when(home != mirror)
                def _(copy=copy):
                    copy.wait_recv()

    def send_back(g):
        for i, home in enumerate(groups[g]):
            if g or i:
                c = pltpu.make_async_remote_copy(
                    src_ref=retbuf.at[home], dst_ref=back.at[me], send_sem=rsend.at[home], recv_sem=rrecv.at[me],
                    device_id={"ep": home}, device_id_type=MESH,
                )
                c.start()
                pending.append(c)

    def wait_back(g):
        for i, frm in enumerate(groups[g]):
            if g or i:
                pltpu.make_async_remote_copy(
                    src_ref=retbuf.at[frm], dst_ref=back.at[frm], send_sem=rsend.at[frm], recv_sem=rrecv.at[frm],
                    device_id={"ep": frm}, device_id_type=MESH,
                ).wait_recv()

    routes = routes_ref[...]
    meta[0:picks, 0:toks] = routes.astype(F32)
    x = x_ref[...]
    gain = gain_ref[...]
    select_rows(0, routes, x)
    pl.semaphore_wait(barrier, m + tp - 1)
    mcopy = to_mirror(meta, metam, 1)
    xcopy = to_mirror(x_ref, xm_ref, 0)
    send_tokens(0, me)
    rw = rw_ref[...]
    scaled = 2.5 * rw / jnp.sum(rw, axis=0, keepdims=True)
    hits, place = places(routes, 0, n)
    weight = jnp.zeros((n, toks), F32)
    for k in range(picks):
        weight = weight + jnp.where(hits[k], scaled[k : k + 1, :], 0.0)
    w_hi = weight.astype(BF16).astype(F32)
    comb_hi, comb_lo = by_slot(place, w_hi), by_slot(place, weight - w_hi)
    rows[...] = jnp.zeros(rows.shape, BF16)
    mcopy.wait_recv()
    routes_m = metam[0:picks, 0:toks].astype(jnp.int32)
    xcopy.wait_recv()
    select_rows(1, routes_m, xm_ref[...])
    send_tokens(1, mirror)

    def start_shared():
        xf = x.astype(F32)
        xg = (xf * gain).astype(BF16)
        ss_own = jnp.sum(xf * xf, axis=1, keepdims=True)
        shsend[...] = jnp.zeros(shsend.shape, F32)
        shsend[0:toks, 2 * fs : 2 * fs + LANES] = jnp.broadcast_to(ss_own, (toks, LANES))
        for name, w, base in (("sg", vg, 0), ("su", vu, fs)):
            loaded(name)
            shsend[0:toks, base : base + fs] = jnp.dot(xg, w[...], preferred_element_type=F32)

    def send_shared():
        return to_tp(shsend, lambda i: shrecv.at[i], lambda i: hsend.at[i], lambda i: hrecv.at[i])

    def finish_shared(copies):
        loaded("sd")
        for c in copies:
            c.wait_recv()
        total = shsend[...]
        for i in range(tp - 1):
            total = total + shrecv[i]
        r_own = lax.rsqrt(total[:, 2 * fs : 2 * fs + 1] / (width * tp) + 1e-06)
        sh_hidden = silu_mul(total[:, 0:fs] * r_own, total[:, fs : 2 * fs] * r_own).astype(BF16)
        shout[...] = jnp.dot(sh_hidden, vd[...], preferred_element_type=F32)

    starts = []
    for g in range(len(groups)):
        starts.append(sum(-(-len(groups[i]) * cap // 8) * 8 for i in range(g)))

    def first_half(g):
        number = len(groups[g])
        count, base = number * cap, starts[g]
        low = -(-count // 16) * 16
        wait_tokens(g)
        for i, home in enumerate(groups[g]):
            packed[pl.ds(i * jc, jc), :] = arrive[home].astype(F32)
        ss = jnp.zeros((count, LANES), F32)
        for j in range(blocks):
            cut = slice(j * LANES, (j + 1) * LANES)
            piece = unpack(j, number)
            ss = ss + piece * piece
            scaled_piece = piece * gain[:, cut]
            hi = scaled_piece.astype(BF16)
            rows[0:count, cut] = hi
            rows[low : low + count, cut] = (scaled_piece - hi.astype(F32)).astype(BF16)
        sssend[base : base + count] = jnp.broadcast_to(jnp.sum(ss, axis=1, keepdims=True), (count, LANES))
        part = pl.ds(base, count)
        all_copies = [to_tp(
            sssend.at[part], lambda i: ssrecv.at[i, part],
            lambda i: qsend.at[i * len(groups) + g], lambda i: qrecv.at[i * len(groups) + g],
        )]
        taken_rows = rows[0 : 2 * low, :]
        for c in range(chunks):
            cut = slice(c * cols, (c + 1) * cols)
            for w, at in ((wg, 0), (wu, cols)):
                v = jnp.dot(taken_rows, w[:, cut], preferred_element_type=F32)
                v = v[0:count] + v[low : low + count]
                mine[g][c, :, at : at + cols] = v
                psend[g][c, :, at : at + cols] = v.astype(BF16)
            at_sem = lambda i: (i * len(groups) + g) * chunks + c
            all_copies.append(to_tp(
                psend[g].at[c], lambda i: precv[g].at[i, c],
                lambda i: tsend.at[at_sem(i)], lambda i: trecv.at[at_sem(i)],
            ))
        return all_copies

    def second_half(g, all_copies):
        number = len(groups[g])
        count, base = number * cap, starts[g]
        for c in all_copies[0]:
            c.wait_recv()
        ss_all = sssend[base : base + count, :]
        for i in range(tp - 1):
            ss_all = ss_all + ssrecv[i, base : base + count, :]
        r = lax.rsqrt(ss_all[:, 0:1] / (width * tp) + 1e-06)
        for c in range(chunks):
            for copy in all_copies[1 + c]:
                copy.wait_recv()
            both = mine[g][c]
            for i in range(tp - 1):
                both = both + precv[g][i, c].astype(F32)
            hidden = silu_mul(both[:, 0:cols] * r, both[:, cols : 2 * cols] * r).astype(BF16)
            part = jnp.dot(hidden, wd[c * cols : (c + 1) * cols, :], preferred_element_type=F32)
            if c == 0:
                acc[0:count, :] = part
            elif c < chunks - 1:
                acc[0:count, :] += part
            else:
                for j in range(blocks):
                    cut = slice(j * LANES, (j + 1) * LANES)
                    pack(acc[0:count, cut] + part[:, cut], j, number)
        for i, home in enumerate(groups[g]):
            retbuf[home] = packed[pl.ds(i * jc, jc), :].astype(BF16)
        send_back(g)

    loaded("eg", "eu")
    state0 = first_half(0)
    start_shared()
    state1 = first_half(1)
    state2 = first_half(2)
    shared = send_shared()
    loaded("ed")
    second_half(0, state0)
    back[me] = retbuf[me]
    second_half(1, state1)
    second_half(2, state2)
    finish_shared(shared)
    for g in range(len(groups)):
        wait_back(g)
    for p in range(n):
        packed[pl.ds(p * jc, jc), :] = back[p].astype(F32)
    for j in range(blocks):
        cut = slice(j * LANES, (j + 1) * LANES)
        piece = unpack(j, n).astype(BF16)
        routed = lax.dot_general(comb_hi, piece, TN, preferred_element_type=F32)
        routed = routed + lax.dot_general(comb_lo, piece, TN, preferred_element_type=F32)
        out_ref[:, cut] = (shout[0:toks, cut] + routed).astype(BF16)
    for c in pending:
        c.wait_send()


def local(tokens, norm_gain, routes, route_weights, eg, eu, ed, sg, su, sd):
    toks, width = tokens.shape
    picks = routes.shape[1]
    n, tp = lax.axis_size("ep"), lax.axis_size("tp")
    cap = max(2, toks * picks // n + 1)
    ff, fs = eg.shape[2], sg.shape[1]
    chunks, pieces = 2, 4
    m, quarter = n // 2, n // 4
    jc = width // LANES * cap
    low = -(-m * cap // 16) * 16
    padded = -(-toks // 16) * 16
    cols = ff // chunks
    others = max(1, tp - 1)
    split = -(-picks // 8) * 8
    sizes = (m, quarter, quarter)
    total_rows = sum(-(-s * cap // 8) * 8 for s in sizes)
    exchanged = []
    for s in sizes:
        exchanged += [
            pltpu.VMEM((chunks, s * cap, 2 * cols), F32),
            pltpu.VMEM((chunks, s * cap, 2 * cols), BF16),
            pltpu.VMEM((others, chunks, s * cap, 2 * cols), BF16),
        ]
    hbm = pl.BlockSpec(memory_space=pl.ANY)
    dma = pltpu.SemaphoreType.DMA
    return pl.pallas_call(
        functools.partial(kernel, n, tp, cap, chunks, pieces),
        out_shape=pltpu.VMEM((toks, width), BF16),
        in_specs=[hbm] * 10,
        out_specs=pl.BlockSpec(memory_space=pltpu.VMEM),
        scratch_shapes=[
            pltpu.VMEM((width, ff), BF16), pltpu.VMEM((width, ff), BF16), pltpu.VMEM((ff, width), BF16),
            pltpu.VMEM((width, fs), BF16), pltpu.VMEM((width, fs), BF16), pltpu.VMEM((fs, width), BF16),
            pltpu.VMEM((toks, width), BF16), pltpu.VMEM((1, width), F32),
            pltpu.VMEM((picks, toks), jnp.int32), pltpu.VMEM((picks, toks), F32),
            pltpu.VMEM((toks, width), BF16),
            pltpu.VMEM((split, LANES), F32), pltpu.VMEM((split, LANES), F32),
            pltpu.VMEM((n * jc, LANES), F32),
            pltpu.VMEM((2, m, jc, LANES), BF16), pltpu.VMEM((n, jc, LANES), BF16),
            pltpu.VMEM((n, jc, LANES), BF16), pltpu.VMEM((n, jc, LANES), BF16),
            pltpu.VMEM((2 * low, width), BF16),
            pltpu.VMEM((total_rows, LANES), F32), pltpu.VMEM((others, total_rows, LANES), F32),
            pltpu.VMEM((padded, 2 * fs + LANES), F32), pltpu.VMEM((others, padded, 2 * fs + LANES), F32),
            pltpu.VMEM((m * cap, width), F32), pltpu.VMEM((padded, width), F32),
            dma((4,)), dma((6 * pieces,)),
            dma((2, m)), dma((n,)), dma((n,)), dma((n,)),
            dma((others * chunks * 3,)), dma((others * chunks * 3,)),
            dma((others * 3,)), dma((others * 3,)), dma((others,)), dma((others,)), dma((2,)), dma((2,)),
        ] + exchanged,
        compiler_params=pltpu.CompilerParams(
            collective_id=0, has_side_effects=True, vmem_limit_bytes=60 * 1024 * 1024
        ),
    )(tokens, norm_gain.reshape(1, width), routes.T, route_weights.T, eg, eu, ed, sg, su, sd)


def solution(mesh):
    placed = (
        P("ep", "tp"),
        P("tp"),
        P("ep", None),
        P("ep", None),
        P("ep", "tp", None),
        P("ep", "tp", None),
        P("ep", None, "tp"),
        P("tp", None),
        P("tp", None),
        P(None, "tp"),
    )
    return jax.shard_map(
        local, mesh=mesh, in_specs=placed, out_specs=P("ep", "tp"), check_vma=False
    )
```

time: 33.4 us -> 29.7 us (0.89)
  the two profiles are of different devices: /device:TPU:0 before, /device:TPU:1 now
where the time goes in v1:
time: 29.7 us; the launch traced here: 29.6 us
  Pallas kernels  28.9 us (97%)
  local copies, waits for them, and re-layouts  0.63 us (2%)
    pallas_call x1, Pallas kernels, local(): pl.pallas_call(functools.partial(kernel, n, tp, cap, chunks, pieces), out...  28.9 us
    unnamed x1, local copies, waits for them, and re-layouts  0.63 us

profile of v1, /device:TPU:1, one launch (start us, length us, event | category | flops | bytes accessed | tf_op | source)
XLA Modules:
  0.0 29.6 jit_solution(16601920906072087222)
XLA Ops:
  0.0 28.9 %shard_map.100 = bf16[12,2048]{1,0:T(8,128)(2,1)S(1)} custom-call(bf16[12,2048]{1,0:T(8,128)(2,1)} %x_hbm.1, f32[1,2048]{1,0:T(1,128)} %bitcast.3, s32[6,12]{1,0:T(8,128)} %bitcast.4, f32[6,12]{1,0:T(8,128)} %bitcast.5, bf16[1,2048,1024]{2,1,0:T(8,128)(2,1)} %eg_hbm.1, bf16[1,2048,1024]{2,1,0:T(8,128)(2,1)} %eu_hbm.1, bf16[1,1024,2048]{2,1,0:T(8,128)(2,1)} %ed_hbm.1, ...), custom_call_target="tpu_custom_call" | custom-call | tf_op jit(solution)/shard_map/pallas_call | solution.py:362
  28.9 0.6 %copy.12 = bf16[12,2048]{1,0:T(8,128)(2,1)} copy(bf16[12,2048]{1,0:T(8,128)(2,1)S(1)} %shard_map.100) | data formatting | bytes 98304

commit v2 on v1

v2 whole, which is shorter than its diff:
```python
import functools

import jax
import jax.numpy as jnp
from jax import lax
from jax.experimental import pallas as pl
from jax.experimental.pallas import tpu as pltpu
from jax.sharding import PartitionSpec as P

MESH = pl.DeviceIdType.MESH
F32 = jnp.float32
BF16 = jnp.bfloat16
LANES = 128
TN = (((0,), (0,)), ((), ()))


def silu_mul(g, u):
    return g / (1.0 + jnp.exp(-g)) * u


def kernel(
    n, tp, cap, chunks,
    x_hbm, gain_hbm, routes_hbm, rw_hbm,
    eg_hbm, eu_hbm, ed_hbm, sg_hbm, su_hbm, sd_hbm,
    out_ref,
    wgu, wd, vg, vu, vd,
    x_ref, gain_ref, routes_ref, rw_ref, xm_ref, meta, metam,
    packed, outbuf, arrive, retbuf, back,
    rows, hid, squares, sssend, ssrecv, shsend, shrecv, acc, shout,
    isem, wsem, dsend, drecv, rsend, rrecv, tsend, trecv, qsend, qrecv, hsend, hrecv, xsend, xrecv, asend, arecv,
    *exchanged,
):
    me = lax.axis_index("ep")
    my_tp = lax.axis_index("tp")
    m, quarter = n // 2, n // 4
    half, inner = me // m, lax.rem(me, m)
    mirror = lax.rem(me + m, n)
    spot = lax.rem(me, quarter)
    bit = lax.rem(me // quarter, 2)
    split_ff = tp == 2
    early = me // quarter == 1
    theirs = 1 - my_tp
    toks, width = x_ref.shape
    picks = routes_ref.shape[0]
    ff = wd.shape[0]
    fs = vg.shape[1]
    blocks = width // LANES
    jc = blocks * cap
    cols = ff // chunks
    mine, psend, precv = exchanged[0::3], exchanged[1::3], exchanged[2::3]

    def mate(i):
        return half * m + lax.rem(inner + i, m)

    def in_quarter(q):
        return [q * quarter + lax.rem(spot + i, quarter) for i in range(quarter)]

    near = [mate(i) for i in range(m)]
    groups = [near, in_quarter(2 * (1 - half)), in_quarter(2 * (1 - half) + 1)]

    barrier = pltpu.get_barrier_semaphore()
    pl.semaphore_signal(barrier, inc=1, device_id={"ep": mirror}, device_id_type=MESH)
    for i in range(1, m):
        pl.semaphore_signal(barrier, inc=1, device_id={"ep": mate(i)}, device_id_type=MESH)
    for i in range(1, tp):
        pl.semaphore_signal(barrier, inc=1, device_id={"tp": lax.rem(my_tp + i, tp)}, device_id_type=MESH)

    small = []
    for i, (src, dst) in enumerate(
        ((routes_hbm, routes_ref), (rw_hbm, rw_ref), (x_hbm, x_ref), (gain_hbm, gain_ref))
    ):
        c = pltpu.make_async_copy(src, dst, isem.at[i])
        c.start()
        small.append(c)
    for c in small:
        c.wait()
    loads = {}
    parts = [("sg", sg_hbm, vg), ("su", su_hbm, vu)]
    for c in range(chunks):
        which = (theirs, my_tp)[c] if split_ff else c
        taken = pl.ds(pl.multiple_of(which * cols, LANES), cols)
        parts.append((f"e{c}", eg_hbm.at[0, :, taken], wgu.at[which, :, 0:cols]))
        parts.append((f"e{c}", eu_hbm.at[0, :, taken], wgu.at[which, :, cols : 2 * cols]))
    parts += [("ed", ed_hbm.at[0], wd), ("sd", sd_hbm, vd)]
    for slot, (name, src, dst) in enumerate(parts):
        c = pltpu.make_async_copy(src, dst, wsem.at[slot])
        c.start()
        loads.setdefault(name, []).append(c)

    def loaded(*names):
        for name in names:
            for c in loads[name]:
                c.wait()

    def places(routes, base, number):
        expert = lax.broadcasted_iota(jnp.int32, (number, toks), 0) + base
        hits = [routes[k : k + 1, :] == expert for k in range(picks)]
        named = jnp.zeros((number, toks), F32)
        for hit in hits:
            named = named + jnp.where(hit, 1.0, 0.0)
        row_i = lax.broadcasted_iota(jnp.int32, (toks, toks), 0)
        col_i = lax.broadcasted_iota(jnp.int32, (toks, toks), 1)
        earlier = jnp.where(row_i < col_i, 1.0, 0.0).astype(BF16)
        before = jnp.dot(named.astype(BF16), earlier, preferred_element_type=F32)
        return hits, jnp.where(named > 0.5, before, -1.0)

    def by_slot(place, v):
        return jnp.concatenate([jnp.where(place == s, v, 0.0) for s in range(cap)], axis=0).astype(BF16)

    def pack(value, j, number):
        for s in range(cap):
            packed[pl.ds(j * cap + s, number, stride=jc), :] = value[s * number : (s + 1) * number, :]

    def unpack(j, number):
        return jnp.concatenate(
            [packed[pl.ds(j * cap + s, number, stride=jc), :] for s in range(cap)], axis=0
        )

    def select_rows(g, routes, x):
        select = by_slot(places(routes, half * m, m)[1], 1.0)
        for j in range(blocks):
            cut = slice(j * LANES, (j + 1) * LANES)
            pack(jnp.dot(select, x[:, cut], preferred_element_type=F32), j, m)
        for p in range(m):
            outbuf[g, p] = packed[pl.ds(p * jc, jc), :].astype(BF16)

    pending = []

    def to_tp(src, dst_of, send_of, recv_of):
        copies = []
        for i in range(1, tp):
            c = pltpu.make_async_remote_copy(
                src_ref=src, dst_ref=dst_of(i - 1), send_sem=send_of(i - 1), recv_sem=recv_of(i - 1),
                device_id={"tp": lax.rem(my_tp + i, tp)}, device_id_type=MESH,
            )
            c.start()
            copies.append(c)
        pending.extend(copies)
        return copies

    def to_mirror(src, dst, at):
        c = pltpu.make_async_remote_copy(
            src_ref=src, dst_ref=dst, send_sem=xsend.at[at], recv_sem=xrecv.at[at],
            device_id={"ep": mirror}, device_id_type=MESH,
        )
        c.start()
        pending.append(c)
        return c

    def token_copies(g, home):
        for i in range(1, m):
            to = lax.rem(inner + i, m)
            pltpu.make_async_remote_copy(
                src_ref=outbuf.at[g, to], dst_ref=arrive.at[home], send_sem=dsend.at[g],
                recv_sem=drecv.at[g * (1 + bit)], device_id={"ep": mate(i)}, device_id_type=MESH,
            ).start()
        arrive[home] = outbuf[g, inner]

    def many(ref, number, send, recv):
        part = ref.at[pl.ds(0, number)]
        return pltpu.make_async_remote_copy(
            src_ref=part, dst_ref=part, send_sem=send, recv_sem=recv,
            device_id={"ep": mirror}, device_id_type=MESH,
        )

    def wait_tokens(g):
        if g == 0:
            many(arrive, m - 1, dsend.at[0], drecv.at[0]).wait_recv()
            return

        @pl.when(bit == g - 1)
        def _():
            many(arrive, quarter - 1, dsend.at[0], drecv.at[g]).wait_recv()

        @pl.when(bit != g - 1)
        def _():
            many(arrive, quarter, dsend.at[0], drecv.at[g]).wait_recv()

    def send_back(g):
        for i, home in enumerate(groups[g]):
            if g or i:
                pltpu.make_async_remote_copy(
                    src_ref=retbuf.at[home], dst_ref=back.at[me], send_sem=rsend.at[g],
                    recv_sem=rrecv.at[1 + bit if g else 0], device_id={"ep": home}, device_id_type=MESH,
                ).start()

    def returned(g):
        return many(back, quarter if g else m - 1, rsend.at[g], rrecv.at[g])

    routes = routes_ref[...]
    meta[0:picks, 0:toks] = routes.astype(F32)
    x = x_ref[...]
    gain = gain_ref[...]
    select_rows(0, routes, x)
    pl.semaphore_wait(barrier, m + tp - 1)
    mcopy = to_mirror(meta, metam, 1)
    xcopy = to_mirror(x_ref, xm_ref, 0)
    token_copies(0, me)
    rw = rw_ref[...]
    scaled = 2.5 * rw / jnp.sum(rw, axis=0, keepdims=True)

    def combiner(base):
        hits, place = places(routes, base, m)
        weight = jnp.zeros((m, toks), F32)
        for k in range(picks):
            weight = weight + jnp.where(hits[k], scaled[k : k + 1, :], 0.0)
        w_hi = weight.astype(BF16).astype(F32)
        return by_slot(place, w_hi), by_slot(place, weight - w_hi)

    combiners = combiner(half * m), combiner((1 - half) * m)
    rows[...] = jnp.zeros(rows.shape, BF16)
    xf = x.astype(F32)
    xg = (xf * gain).astype(BF16)
    ss_own = jnp.sum(xf * xf, axis=1, keepdims=True)
    shsend[...] = jnp.zeros(shsend.shape, F32)
    shsend[0:toks, 2 * fs : 2 * fs + LANES] = jnp.broadcast_to(ss_own, (toks, LANES))
    for name, w, base in (("sg", vg, 0), ("su", vu, fs)):
        loaded(name)
        shsend[0:toks, base : base + fs] = jnp.dot(xg, w[...], preferred_element_type=F32)
    shared = to_tp(shsend, lambda i: shrecv.at[i], lambda i: hsend.at[i], lambda i: hrecv.at[i])
    mcopy.wait_recv()
    xcopy.wait_recv()
    select_rows(1, metam[0:picks, 0:toks].astype(jnp.int32), xm_ref[...])
    token_copies(1, mirror)

    def finish_shared(copies):
        loaded("sd")
        for c in copies:
            c.wait_recv()
        total = shsend[...]
        for i in range(tp - 1):
            total = total + shrecv[i]
        r_own = lax.rsqrt(total[:, 2 * fs : 2 * fs + 1] / (width * tp) + 1e-06)
        sh_hidden = silu_mul(total[:, 0:fs] * r_own, total[:, fs : 2 * fs] * r_own).astype(BF16)
        shout[...] = jnp.dot(sh_hidden, vd[...], preferred_element_type=F32)

    def first_half(g):
        number = len(groups[g])
        count = number * cap
        low = -(-count // 16) * 16
        wait_tokens(g)
        for i, home in enumerate(groups[g]):
            packed[pl.ds(i * jc, jc), :] = arrive[home].astype(F32)
        ss = jnp.zeros((count, LANES), F32)
        for j in range(blocks):
            cut = slice(j * LANES, (j + 1) * LANES)
            piece = unpack(j, number)
            ss = ss + piece * piece
            scaled_piece = piece * gain[:, cut]
            hi = scaled_piece.astype(BF16)
            rows[0:count, cut] = hi
            rows[low : low + count, cut] = (scaled_piece - hi.astype(F32)).astype(BF16)
        squares[0:count, :] = jnp.broadcast_to(jnp.sum(ss, axis=1, keepdims=True), (count, LANES))
        sssend[g] = squares[...].T[0:8, :]
        all_copies = [to_tp(
            sssend.at[g], lambda i: ssrecv.at[i, g],
            lambda i: qsend.at[i * len(groups) + g], lambda i: qrecv.at[i * len(groups) + g],
        )]
        taken_rows = rows[0 : 2 * low, :]
        for c in range(chunks):
            loaded_once(c)
            own = split_ff and g == 0 and c > 0
            which = (theirs, my_tp)[c] if split_ff else c
            v = jnp.dot(taken_rows, wgu[which], preferred_element_type=F32)
            v = v[0:count] + v[low : low + count]
            mine[g][c] = v
            if own:
                continue
            psend[g][c] = v.astype(BF16)
            at_sem = lambda i: (i * len(groups) + g) * chunks + c
            all_copies.append(to_tp(
                psend[g].at[c], lambda i: precv[g].at[i, c],
                lambda i: tsend.at[at_sem(i)], lambda i: trecv.at[at_sem(i)],
            ))
        return all_copies

    def scale(g, copies):
        for c in copies:
            c.wait_recv()
        ss_all = sssend[g]
        for i in range(tp - 1):
            ss_all = ss_all + ssrecv[i, g]
        r_all = lax.rsqrt(ss_all / (width * tp) + 1e-06)
        return jnp.broadcast_to(r_all[0:1, :], squares.shape[::-1]).T[0 : len(groups[g]) * cap, 0:1]

    def activate(both, r):
        return silu_mul(both[:, 0:cols] * r, both[:, cols : 2 * cols] * r).astype(BF16)

    def deliver(g, value_of):
        number = len(groups[g])
        for j in range(blocks):
            pack(value_of(slice(j * LANES, (j + 1) * LANES)), j, number)
        for i, home in enumerate(groups[g]):
            retbuf[home] = packed[pl.ds(i * jc, jc), :].astype(BF16)
        send_back(g)
        if g == 0:
            back[me] = retbuf[me]

    def hidden_copy():
        return pltpu.make_async_remote_copy(
            src_ref=hid.at[my_tp], dst_ref=hid.at[my_tp], send_sem=asend.at[0], recv_sem=arecv.at[0],
            device_id={"tp": theirs}, device_id_type=MESH,
        )

    def hidden_half(all_copies):
        r = scale(0, all_copies[0])
        for c in all_copies[1]:
            c.wait_recv()
        hid[my_tp] = activate(mine[0][1] + precv[0][0, 0].astype(F32), r)
        hidden_copy().start()

    def out_half():
        hidden_copy().wait_recv()
        acc[0 : m * cap, :] = jnp.dot(hid[0], wd[0:cols, :], preferred_element_type=F32)
        part = jnp.dot(hid[1], wd[cols : 2 * cols, :], preferred_element_type=F32)
        deliver(0, lambda cut: acc[0 : m * cap, cut] + part[:, cut])

    def second_half(g, all_copies):
        count = len(groups[g]) * cap
        r = scale(g, all_copies[0])
        for c in range(chunks):
            for copy in all_copies[1 + c]:
                copy.wait_recv()
            which = (my_tp, theirs)[c] if split_ff else c
            both = mine[g][1 - c if split_ff else c]
            for i in range(tp - 1):
                both = both + precv[g][i, c].astype(F32)
            hidden = activate(both, r)
            part = jnp.dot(hidden, wd[pl.ds(pl.multiple_of(which * cols, LANES), cols), :], preferred_element_type=F32)
            if c == 0:
                acc[0:count, :] = part
            elif c < chunks - 1:
                acc[0:count, :] += part
            else:
                deliver(g, lambda cut: acc[0:count, cut] + part[:, cut])

    fetched = set()

    def loaded_once(c):
        if c not in fetched:
            fetched.add(c)
            loaded(f"e{c}")

    state0 = first_half(0)
    if split_ff:
        pl.when(early)(lambda: hidden_half(state0))
    state1 = first_half(1)
    state2 = first_half(2)
    loaded("ed")
    if split_ff:
        pl.when(jnp.logical_not(early))(lambda: hidden_half(state0))
        pl.when(early)(out_half)
    else:
        second_half(0, state0)
    second_half(1, state1)
    second_half(2, state2)
    if split_ff:
        pl.when(jnp.logical_not(early))(out_half)
    finish_shared(shared)

    def combined(base, pair):
        for p in range(m):
            packed[pl.ds(p * jc, jc), :] = back[base + p].astype(F32)
        for j in range(blocks):
            cut = slice(j * LANES, (j + 1) * LANES)
            piece = unpack(j, m).astype(BF16)
            routed = lax.dot_general(pair[0], piece, TN, preferred_element_type=F32)
            yield cut, routed + lax.dot_general(pair[1], piece, TN, preferred_element_type=F32)

    returned(0).wait_recv()
    for cut, routed in combined(half * m, combiners[0]):
        shout[0:toks, cut] += routed
    returned(1).wait_recv()
    returned(2).wait_recv()
    for cut, routed in combined((1 - half) * m, combiners[1]):
        out_ref[:, cut] = (shout[0:toks, cut] + routed).astype(BF16)
    for c in pending:
        c.wait_send()
    for g in range(2):
        many(arrive, m - 1, dsend.at[g], drecv.at[g]).wait_send()
    for g in range(len(groups)):
        returned(g).wait_send()
    if split_ff:
        hidden_copy().wait_send()


def local(tokens, norm_gain, routes, route_weights, eg, eu, ed, sg, su, sd):
    toks, width = tokens.shape
    picks = routes.shape[1]
    n, tp = lax.axis_size("ep"), lax.axis_size("tp")
    cap = max(2, toks * picks // n + 1)
    ff, fs = eg.shape[2], sg.shape[1]
    chunks = 2
    m, quarter = n // 2, n // 4
    jc = width // LANES * cap
    low = -(-m * cap // 16) * 16
    padded = -(-toks // 16) * 16
    cols = ff // chunks
    others = max(1, tp - 1)
    split = -(-picks // 8) * 8
    sizes = (m, quarter, quarter)
    slots = -(-m * cap // LANES) * LANES
    exchanged = []
    for s in sizes:
        exchanged += [
            pltpu.VMEM((chunks, s * cap, 2 * cols), F32),
            pltpu.VMEM((chunks, s * cap, 2 * cols), BF16),
            pltpu.VMEM((others, chunks, s * cap, 2 * cols), BF16),
        ]
    hbm = pl.BlockSpec(memory_space=pl.ANY)
    dma = pltpu.SemaphoreType.DMA
    return pl.pallas_call(
        functools.partial(kernel, n, tp, cap, chunks),
        out_shape=pltpu.VMEM((toks, width), BF16),
        in_specs=[hbm] * 10,
        out_specs=pl.BlockSpec(memory_space=pltpu.VMEM),
        scratch_shapes=[
            pltpu.VMEM((chunks, width, 2 * cols), BF16), pltpu.VMEM((ff, width), BF16),
            pltpu.VMEM((width, fs), BF16), pltpu.VMEM((width, fs), BF16), pltpu.VMEM((fs, width), BF16),
            pltpu.VMEM((toks, width), BF16), pltpu.VMEM((1, width), F32),
            pltpu.VMEM((picks, toks), jnp.int32), pltpu.VMEM((picks, toks), F32),
            pltpu.VMEM((toks, width), BF16),
            pltpu.VMEM((split, LANES), F32), pltpu.VMEM((split, LANES), F32),
            pltpu.VMEM((n * jc, LANES), F32),
            pltpu.VMEM((2, m, jc, LANES), BF16), pltpu.VMEM((n, jc, LANES), BF16),
            pltpu.VMEM((n, jc, LANES), BF16), pltpu.VMEM((n, jc, LANES), BF16),
            pltpu.VMEM((2 * low, width), BF16), pltpu.VMEM((chunks, m * cap, cols), BF16),
            pltpu.VMEM((slots, LANES), F32),
            pltpu.VMEM((3, 8, slots), F32), pltpu.VMEM((others, 3, 8, slots), F32),
            pltpu.VMEM((padded, 2 * fs + LANES), F32), pltpu.VMEM((others, padded, 2 * fs + LANES), F32),
            pltpu.VMEM((m * cap, width), F32), pltpu.VMEM((padded, width), F32),
            dma((4,)), dma((4 + 2 * chunks,)),
            dma((2,)), dma((3,)), dma((3,)), dma((3,)),
            dma((others * chunks * 3,)), dma((others * chunks * 3,)),
            dma((others * 3,)), dma((others * 3,)), dma((others,)), dma((others,)), dma((2,)), dma((2,)),
            dma((1,)), dma((1,)),
        ] + exchanged,
        compiler_params=pltpu.CompilerParams(
            collective_id=0, has_side_effects=True, vmem_limit_bytes=60 * 1024 * 1024
        ),
    )(tokens, norm_gain.reshape(1, width), routes.T, route_weights.T, eg, eu, ed, sg, su, sd)


def solution(mesh):
    placed = (
        P("ep", "tp"),
        P("tp"),
        P("ep", None),
        P("ep", None),
        P("ep", "tp", None),
        P("ep", "tp", None),
        P("ep", None, "tp"),
        P("tp", None),
        P("tp", None),
        P(None, "tp"),
    )
    return jax.shard_map(
        local, mesh=mesh, in_specs=placed, out_specs=P("ep", "tp"), check_vma=False
    )
```

time: 29.7 us -> 28.8 us (0.970)
  the two profiles are of different devices: /device:TPU:1 before, /device:TPU:0 now
where the time goes in v2:
time: 28.8 us; the launch traced here: 28.3 us
  Pallas kernels  27.7 us (96%)
  local copies, waits for them, and re-layouts  0.63 us (2%)
    pallas_call x1, Pallas kernels, local(): pl.pallas_call(functools.partial(kernel, n, tp, cap, chunks), out_shape=p...  27.7 us
    unnamed x1, local copies, waits for them, and re-layouts  0.63 us

profile of v2, /device:TPU:0, one launch (start us, length us, event | category | flops | bytes accessed | tf_op | source)
XLA Modules:
  0.0 28.3 jit_solution(14793800235964327485)
XLA Ops:
  0.0 27.7 %shard_map.100 = bf16[12,2048]{1,0:T(8,128)(2,1)S(1)} custom-call(bf16[12,2048]{1,0:T(8,128)(2,1)} %x_hbm.1, f32[1,2048]{1,0:T(1,128)} %bitcast.3, s32[6,12]{1,0:T(8,128)} %bitcast.4, f32[6,12]{1,0:T(8,128)} %bitcast.5, bf16[1,2048,1024]{2,1,0:T(8,128)(2,1)} %eg_hbm.1, bf16[1,2048,1024]{2,1,0:T(8,128)(2,1)} %eu_hbm.1, bf16[1,1024,2048]{2,1,0:T(8,128)(2,1)} %ed_hbm.1, ...), custom_call_target="tpu_custom_call" | custom-call | tf_op jit(solution)/shard_map/pallas_call | solution.py:412
  27.7 0.6 %copy.12 = bf16[12,2048]{1,0:T(8,128)(2,1)} copy(bf16[12,2048]{1,0:T(8,128)(2,1)S(1)} %shard_map.100) | data formatting | bytes 98304

commit v3 on v2

--- a/solution.py
+++ b/solution.py
@@ -38,7 +38,6 @@
     spot = lax.rem(me, quarter)
     bit = lax.rem(me // quarter, 2)
     split_ff = tp == 2
-    early = me // quarter == 1
     theirs = 1 - my_tp
     toks, width = x_ref.shape
     picks = routes_ref.shape[0]
@@ -56,7 +55,9 @@
         return [q * quarter + lax.rem(spot + i, quarter) for i in range(quarter)]
 
     near = [mate(i) for i in range(m)]
-    groups = [near, in_quarter(2 * (1 - half)), in_quarter(2 * (1 - half) + 1)]
+    groups = [near, in_quarter(3 * (1 - half)), in_quarter(2 - half)]
+    mirror_group = 1 + lax.rem(bit + 1 - half, 2)
+    group_there = 1 + lax.rem(bit + half, 2)
 
     barrier = pltpu.get_barrier_semaphore()
     pl.semaphore_signal(barrier, inc=1, device_id={"ep": mirror}, device_id_type=MESH)
@@ -152,7 +153,7 @@
             to = lax.rem(inner + i, m)
             pltpu.make_async_remote_copy(
                 src_ref=outbuf.at[g, to], dst_ref=arrive.at[home], send_sem=dsend.at[g],
-                recv_sem=drecv.at[g * (1 + bit)], device_id={"ep": mate(i)}, device_id_type=MESH,
+                recv_sem=drecv.at[g * mirror_group], device_id={"ep": mate(i)}, device_id_type=MESH,
             ).start()
         arrive[home] = outbuf[g, inner]
 
@@ -168,11 +169,11 @@
             many(arrive, m - 1, dsend.at[0], drecv.at[0]).wait_recv()
             return
 
-        @pl.when(bit == g - 1)
+        @pl.when(mirror_group == g)
         def _():
             many(arrive, quarter - 1, dsend.at[0], drecv.at[g]).wait_recv()
 
-        @pl.when(bit != g - 1)
+        @pl.when(mirror_group != g)
         def _():
             many(arrive, quarter, dsend.at[0], drecv.at[g]).wait_recv()
 
@@ -181,7 +182,7 @@
             if g or i:
                 pltpu.make_async_remote_copy(
                     src_ref=retbuf.at[home], dst_ref=back.at[me], send_sem=rsend.at[g],
-                    recv_sem=rrecv.at[1 + bit if g else 0], device_id={"ep": home}, device_id_type=MESH,
+                    recv_sem=rrecv.at[group_there if g else 0], device_id={"ep": home}, device_id_type=MESH,
                 ).start()
 
     def returned(g):
@@ -341,21 +342,23 @@
             fetched.add(c)
             loaded(f"e{c}")
 
+    def only(where, step):
+        if split_ff:
+            pl.when(where)(step)
+
+    lower, upper = half == 0, half == 1
     state0 = first_half(0)
-    if split_ff:
-        pl.when(early)(lambda: hidden_half(state0))
     state1 = first_half(1)
+    only(lower, lambda: hidden_half(state0))
     state2 = first_half(2)
+    only(upper, lambda: hidden_half(state0))
     loaded("ed")
-    if split_ff:
-        pl.when(jnp.logical_not(early))(lambda: hidden_half(state0))
-        pl.when(early)(out_half)
-    else:
+    if not split_ff:
         second_half(0, state0)
     second_half(1, state1)
+    only(lower, out_half)
     second_half(2, state2)
-    if split_ff:
-        pl.when(jnp.logical_not(early))(out_half)
+    only(upper, out_half)
     finish_shared(shared)
 
     def combined(base, pair):

time: 28.8 us -> 27.6 us (0.958)
  Pallas kernels: 27.7 us -> 26.5 us
    pallas_call x1, Pallas kernels: 27.7 us -> 26.5 us  [local(): pl.pallas_call(functools.partial(kernel, n, tp, cap, chunks), out_shape=p...]
where the time goes in v3:
time: 27.6 us; the launch traced here: 27.2 us
  Pallas kernels  26.5 us (96%)
  local copies, waits for them, and re-layouts  0.63 us (2%)
    pallas_call x1, Pallas kernels, local(): pl.pallas_call(functools.partial(kernel, n, tp, cap, chunks), out_shape=p...  26.5 us
    unnamed x1, local copies, waits for them, and re-layouts  0.63 us

profile of v3, /device:TPU:0, one launch (start us, length us, event | category | flops | bytes accessed | tf_op | source)
XLA Modules:
  0.0 27.2 jit_solution(14434159570543946805)
XLA Ops:
  0.0 26.5 %shard_map.100 = bf16[12,2048]{1,0:T(8,128)(2,1)S(1)} custom-call(bf16[12,2048]{1,0:T(8,128)(2,1)} %x_hbm.1, f32[1,2048]{1,0:T(1,128)} %bitcast.3, s32[6,12]{1,0:T(8,128)} %bitcast.4, f32[6,12]{1,0:T(8,128)} %bitcast.5, bf16[1,2048,1024]{2,1,0:T(8,128)(2,1)} %eg_hbm.1, bf16[1,2048,1024]{2,1,0:T(8,128)(2,1)} %eu_hbm.1, bf16[1,1024,2048]{2,1,0:T(8,128)(2,1)} %ed_hbm.1, ...), custom_call_target="tpu_custom_call" | custom-call | tf_op jit(solution)/shard_map/pallas_call | solution.py:415
  26.5 0.6 %copy.12 = bf16[12,2048]{1,0:T(8,128)(2,1)} copy(bf16[12,2048]{1,0:T(8,128)(2,1)S(1)} %shard_map.100) | data formatting | bytes 98304

commit v4 on v3

--- a/solution.py
+++ b/solution.py
@@ -52,7 +52,7 @@
         return half * m + lax.rem(inner + i, m)
 
     def in_quarter(q):
-        return [q * quarter + lax.rem(spot + i, quarter) for i in range(quarter)]
+        return [q * quarter + i for i in range(quarter)]
 
     near = [mate(i) for i in range(m)]
     groups = [near, in_quarter(3 * (1 - half)), in_quarter(2 - half)]
@@ -200,15 +200,16 @@
     rw = rw_ref[...]
     scaled = 2.5 * rw / jnp.sum(rw, axis=0, keepdims=True)
 
-    def combiner(base):
-        hits, place = places(routes, base, m)
-        weight = jnp.zeros((m, toks), F32)
+    def combiner(base, number):
+        hits, place = places(routes, base, number)
+        weight = jnp.zeros((number, toks), F32)
         for k in range(picks):
             weight = weight + jnp.where(hits[k], scaled[k : k + 1, :], 0.0)
         w_hi = weight.astype(BF16).astype(F32)
         return by_slot(place, w_hi), by_slot(place, weight - w_hi)
 
-    combiners = combiner(half * m), combiner((1 - half) * m)
+    bases = half * m, 3 * (1 - half) * quarter, (2 - half) * quarter
+    combiners = [combiner(base, len(group)) for base, group in zip(bases, groups)]
     rows[...] = jnp.zeros(rows.shape, BF16)
     xf = x.astype(F32)
     xg = (xf * gain).astype(BF16)
@@ -219,10 +220,13 @@
         loaded(name)
         shsend[0:toks, base : base + fs] = jnp.dot(xg, w[...], preferred_element_type=F32)
     shared = to_tp(shsend, lambda i: shrecv.at[i], lambda i: hsend.at[i], lambda i: hrecv.at[i])
-    mcopy.wait_recv()
-    xcopy.wait_recv()
-    select_rows(1, metam[0:picks, 0:toks].astype(jnp.int32), xm_ref[...])
-    token_copies(1, mirror)
+    def serve_mirror():
+        mcopy.wait_recv()
+        xcopy.wait_recv()
+        select_rows(1, metam[0:picks, 0:toks].astype(jnp.int32), xm_ref[...])
+        token_copies(1, mirror)
+
+    pl.when(me >= quarter)(serve_mirror)
 
     def finish_shared(copies):
         loaded("sd")
@@ -348,6 +352,7 @@
 
     lower, upper = half == 0, half == 1
     state0 = first_half(0)
+    pl.when(me < quarter)(serve_mirror)
     state1 = first_half(1)
     only(lower, lambda: hidden_half(state0))
     state2 = first_half(2)
@@ -361,22 +366,24 @@
     only(upper, out_half)
     finish_shared(shared)
 
-    def combined(base, pair):
-        for p in range(m):
-            packed[pl.ds(p * jc, jc), :] = back[base + p].astype(F32)
+    def combined(g):
+        number = len(groups[g])
+        for p in range(number):
+            packed[pl.ds(p * jc, jc), :] = back[bases[g] + p].astype(F32)
         for j in range(blocks):
             cut = slice(j * LANES, (j + 1) * LANES)
-            piece = unpack(j, m).astype(BF16)
-            routed = lax.dot_general(pair[0], piece, TN, preferred_element_type=F32)
-            yield cut, routed + lax.dot_general(pair[1], piece, TN, preferred_element_type=F32)
-
-    returned(0).wait_recv()
-    for cut, routed in combined(half * m, combiners[0]):
-        shout[0:toks, cut] += routed
-    returned(1).wait_recv()
-    returned(2).wait_recv()
-    for cut, routed in combined((1 - half) * m, combiners[1]):
-        out_ref[:, cut] = (shout[0:toks, cut] + routed).astype(BF16)
+            piece = unpack(j, number).astype(BF16)
+            routed = lax.dot_general(combiners[g][0], piece, TN, preferred_element_type=F32)
+            routed = routed + lax.dot_general(combiners[g][1], piece, TN, preferred_element_type=F32)
+            yield cut, shout[0:toks, cut] + routed
+
+    for g in range(len(groups)):
+        returned(g).wait_recv()
+        for cut, value in combined(g):
+            if g < len(groups) - 1:
+                shout[0:toks, cut] = value
+            else:
+                out_ref[:, cut] = value.astype(BF16)
     for c in pending:
         c.wait_send()
     for g in range(2):

time: 27.6 us -> 26.8 us (0.971)
  Pallas kernels: 26.5 us -> 25.8 us
    pallas_call x1, Pallas kernels: 26.5 us -> 25.8 us  [local(): pl.pallas_call(functools.partial(kernel, n, tp, cap, chunks), out_shape=p...]
where the time goes in v4:
time: 26.8 us; the launch traced here: 26.4 us
  Pallas kernels  25.8 us (96%)
  local copies, waits for them, and re-layouts  0.63 us (2%)
    pallas_call x1, Pallas kernels, local(): pl.pallas_call(functools.partial(kernel, n, tp, cap, chunks), out_shape=p...  25.8 us
    unnamed x1, local copies, waits for them, and re-layouts  0.63 us

profile of v4, /device:TPU:0, one launch (start us, length us, event | category | flops | bytes accessed | tf_op | source)
XLA Modules:
  0.0 26.4 jit_solution(9166258732795726119)
XLA Ops:
  0.0 25.8 %shard_map.100 = bf16[12,2048]{1,0:T(8,128)(2,1)S(1)} custom-call(bf16[12,2048]{1,0:T(8,128)(2,1)} %x_hbm.1, f32[1,2048]{1,0:T(1,128)} %bitcast.3, s32[6,12]{1,0:T(8,128)} %bitcast.4, f32[6,12]{1,0:T(8,128)} %bitcast.5, bf16[1,2048,1024]{2,1,0:T(8,128)(2,1)} %eg_hbm.1, bf16[1,2048,1024]{2,1,0:T(8,128)(2,1)} %eu_hbm.1, bf16[1,1024,2048]{2,1,0:T(8,128)(2,1)} %ed_hbm.1, ...), custom_call_target="tpu_custom_call" | custom-call | tf_op jit(solution)/shard_map/pallas_call | solution.py:422
  25.8 0.6 %copy.12 = bf16[12,2048]{1,0:T(8,128)(2,1)} copy(bf16[12,2048]{1,0:T(8,128)(2,1)S(1)} %shard_map.100) | data formatting | bytes 98304

commit v5 on v4

--- a/solution.py
+++ b/solution.py
@@ -377,7 +377,7 @@
             routed = routed + lax.dot_general(combiners[g][1], piece, TN, preferred_element_type=F32)
             yield cut, shout[0:toks, cut] + routed
 
-    for g in range(len(groups)):
+    for g in (1, 0, 2):
         returned(g).wait_recv()
         for cut, value in combined(g):
             if g < len(groups) - 1:

time: 26.8 us -> 26.7 us (level)
  the two profiles are of different devices: /device:TPU:0 before, /device:TPU:19 now
where the time goes in v5:
time: 26.7 us; the launch traced here: 26.6 us
  Pallas kernels  25.9 us (97%)
  local copies, waits for them, and re-layouts  0.63 us (2%)
    pallas_call x1, Pallas kernels, local(): pl.pallas_call(functools.partial(kernel, n, tp, cap, chunks), out_shape=p...  25.9 us
    unnamed x1, local copies, waits for them, and re-layouts  0.63 us

profile of v5, /device:TPU:19, one launch (start us, length us, event | category | flops | bytes accessed | tf_op | source)
XLA Modules:
  0.0 26.6 jit_solution(3044549235280126077)
XLA Ops:
  0.0 25.9 %shard_map.100 = bf16[12,2048]{1,0:T(8,128)(2,1)S(1)} custom-call(bf16[12,2048]{1,0:T(8,128)(2,1)} %x_hbm.1, f32[1,2048]{1,0:T(1,128)} %bitcast.3, s32[6,12]{1,0:T(8,128)} %bitcast.4, f32[6,12]{1,0:T(8,128)} %bitcast.5, bf16[1,2048,1024]{2,1,0:T(8,128)(2,1)} %eg_hbm.1, bf16[1,2048,1024]{2,1,0:T(8,128)(2,1)} %eu_hbm.1, bf16[1,1024,2048]{2,1,0:T(8,128)(2,1)} %ed_hbm.1, ...), custom_call_target="tpu_custom_call" | custom-call | tf_op jit(solution)/shard_map/pallas_call | solution.py:422
  25.9 0.6 %copy.12 = bf16[12,2048]{1,0:T(8,128)(2,1)} copy(bf16[12,2048]{1,0:T(8,128)(2,1)S(1)} %shard_map.100) | data formatting | bytes 98304
